TPU v7x, 32 devices: a whole 2x2x4 slice. The times are simulated.
32 devices in a mesh: ep: 8 (over z, y), tp: 4 (over x, core).
Axes of the slice: x: 2, y: 2, z: 4, core: 2. Of those that a mesh axis runs over, the one named last changes fastest.
Arguments:
- hidden: bfloat16 [256, 2048], P('ep')
- norm_gains: float32 [4, 2048], replicated, may hold values from 0.1 to 1.9
- w_query: bfloat16 [2048, 1024], P(None, 'tp'), may hold values from -0.125 to 0.125
- w_key: bfloat16 [2048, 1024], P(None, 'tp'), may hold values from -0.125 to 0.125
- w_value: bfloat16 [2048, 1024], P(None, 'tp'), may hold values from -0.125 to 0.125
- w_outgate: bfloat16 [2048, 1024], P(None, 'tp'), may hold values from -0.125 to 0.125
- w_input_gate: bfloat16 [2048, 8], replicated, may hold values from -0.125 to 0.125
- w_forget_gate: bfloat16 [2048, 8], replicated, may hold values from -0.125 to 0.125
- forget_bias: float32 [8], replicated, may hold values from -1 to 4
- w_mix_out: bfloat16 [1024, 2048], P('tp')
- state_matrix: float32 [256, 8, 128, 128], P('ep', 'tp'), may hold values from -0.6 to 0.6
- state_norm: float32 [256, 8, 128], P('ep', 'tp'), may hold values from -0.6 to 0.6
- state_max: float32 [256, 8], P('ep', 'tp'), may hold values from -4 to 4
- routes: int32 [256, 2], P('ep'), may hold values from 0 to 7, all different within a row; in each aligned block of 32 rows (0 to 31, 32 to 63, ...) at most 16 rows name the same one
- route_scores: float32 [256, 2], P('ep'), may hold values from 0.1 to 1
- expert_gate: bfloat16 [8, 2048, 3584], P('ep', None, 'tp'), may hold values from -0.125 to 0.125
- expert_up: bfloat16 [8, 2048, 3584], P('ep', None, 'tp'), may hold values from -0.125 to 0.125
- expert_down: bfloat16 [8, 3584, 2048], P('ep', 'tp')
- dense_gate: bfloat16 [2048, 5632], P('tp', 'ep'), may hold values from -0.125 to 0.125
- dense_up: bfloat16 [2048, 5632], P('tp', 'ep'), may hold values from -0.125 to 0.125
- dense_down: bfloat16 [5632, 2048], P('ep', 'tp')
- dense_mix: float32 [2048], replicated, may hold values from -0.25 to 0.25
Outputs:
- new_hidden: bfloat16 [256, 2048], P('ep', 'tp')
- new_matrix: float32 [256, 8, 128, 128], P('ep', 'tp')
- new_norm: float32 [256, 8, 128], P('ep', 'tp')
- new_max: float32 [256, 8], P('ep', 'tp')
Inputs may be any that keep to these rules, and one draw needn't show every extreme that they name: `routes`: each row names 2 different experts. Among the rows of one index of ep (an aligned block of 32 rows) no expert is named by more than 16 rows, and in every draw some expert is named by exactly 16 rows of some block.
All inputs are finite; a program needn't handle non-finite values.
Results may differ from a plain program's by a relative error of at most 0.02.
Values may be sent and summed in bfloat16 or wider, within the bound.
No kernel may reach another device: no remote copies, remote signals or barrier semaphores. Data moves between devices by JAX's collectives and lax.ppermute only.
A program may use at most 128 MiB of HBM per device.

v0:
```python
import jax
import jax.numpy as jnp
from jax import lax
from jax.sharding import PartitionSpec as P

EPS = 1e-06


def settle(values):
    return lax.optimization_barrier(values.astype(jnp.bfloat16)).astype(jnp.float32)


def local(
    hidden,
    norm_gains,
    w_query,
    w_key,
    w_value,
    w_outgate,
    w_input_gate,
    w_forget_gate,
    forget_bias,
    w_mix_out,
    state_matrix,
    state_norm,
    state_max,
    routes,
    route_scores,
    expert_gate,
    expert_up,
    expert_down,
    dense_gate,
    dense_up,
    dense_down,
    dense_mix,
):
    tp_count = lax.axis_size("tp")
    ep_count = lax.axis_size("ep")
    tp_place = lax.axis_index("tp")
    seq_local, width = hidden.shape
    heads_local = state_matrix.shape[1]
    head_width = state_matrix.shape[2]
    part_width = width // tp_count
    feature_first = tp_place * part_width
    start_f = hidden.astype(jnp.float32)
    normed_in = (
        start_f
        * lax.rsqrt(jnp.mean(start_f * start_f, axis=-1, keepdims=True) + EPS)
        * norm_gains[0]
    ).astype(jnp.bfloat16)
    query_f = jnp.dot(normed_in, w_query, preferred_element_type=jnp.float32)
    key_f = jnp.dot(normed_in, w_key, preferred_element_type=jnp.float32)
    value_f = jnp.dot(normed_in, w_value, preferred_element_type=jnp.float32)
    gate_f = jnp.dot(normed_in, w_outgate, preferred_element_type=jnp.float32)
    head_first = tp_place * heads_local
    input_weight = lax.dynamic_slice_in_dim(w_input_gate, head_first, heads_local, 1)
    forget_weight = lax.dynamic_slice_in_dim(w_forget_gate, head_first, heads_local, 1)
    forget_local = lax.dynamic_slice_in_dim(forget_bias, head_first, heads_local, 0)
    in_gate = jnp.dot(normed_in, input_weight, preferred_element_type=jnp.float32)
    log_forget = jax.nn.log_sigmoid(
        jnp.dot(normed_in, forget_weight, preferred_element_type=jnp.float32) + forget_local
    )
    query = settle(query_f).reshape(seq_local, heads_local, head_width)
    keys = settle(key_f).reshape(seq_local, heads_local, head_width) * head_width ** (-0.5)
    values = settle(value_f).reshape(seq_local, heads_local, head_width)
    carried = log_forget + state_max
    new_max = jnp.maximum(carried, in_gate)
    keep = jnp.exp(carried - new_max)
    write = jnp.exp(in_gate - new_max)
    written = write[:, :, None] * keys
    new_matrix = (
        keep[:, :, None, None] * state_matrix + written[:, :, :, None] * values[:, :, None, :]
    )
    new_norm = keep[:, :, None] * state_norm + written
    numer = jnp.einsum("shd,shdv->shv", query, new_matrix)
    denom = jnp.einsum("shd,shd->sh", query, new_norm)
    read = numer / jnp.maximum(jnp.abs(denom), jnp.exp(-new_max))[:, :, None]
    mixed = (
        jax.nn.sigmoid(settle(gate_f)) * read.reshape(seq_local, heads_local * head_width)
    ).astype(jnp.bfloat16)
    branch_terms = settle(jnp.dot(mixed, w_mix_out, preferred_element_type=jnp.float32))
    branch = settle(
        lax.psum_scatter(
            branch_terms.astype(jnp.bfloat16), "tp", scatter_dimension=1, tiled=True
        ).astype(jnp.float32)
    )
    start_part = lax.dynamic_slice_in_dim(start_f, feature_first, part_width, 1)
    gain_rows = lax.dynamic_slice_in_dim(norm_gains, feature_first, part_width, 1)
    lifted = gain_rows[1] * branch
    mix_weight = gain_rows[2] * lax.dynamic_slice_in_dim(dense_mix, feature_first, part_width, 0)
    branch_sq, start_sq, cross_sum, lifted_sq, start_dot, lifted_dot = lax.psum(
        (
            jnp.sum(branch * branch, axis=-1),
            jnp.sum(start_part * start_part, axis=-1),
            jnp.sum(start_part * lifted, axis=-1),
            jnp.sum(lifted * lifted, axis=-1),
            jnp.sum(start_part * mix_weight, axis=-1),
            jnp.sum(lifted * mix_weight, axis=-1),
        ),
        "tp",
    )
    branch_scale = lax.rsqrt(branch_sq / width + EPS)
    residual_f = start_part + lifted * branch_scale[:, None]
    resid_sq = start_sq + 2.0 * branch_scale * cross_sum + branch_scale * branch_scale * lifted_sq
    gate_dot = start_dot + branch_scale * lifted_dot
    scale_two = lax.rsqrt(resid_sq / width + EPS)
    mix_gate = jax.nn.sigmoid(scale_two * gate_dot)
    residual = settle(residual_f)
    normed = (residual_f * scale_two[:, None] * gain_rows[2]).astype(jnp.bfloat16)
    rows_in = lax.all_gather(normed, "ep", axis=0, tiled=True)
    dense_pre = jnp.concatenate(
        [
            jnp.dot(rows_in, dense_gate, preferred_element_type=jnp.float32),
            jnp.dot(rows_in, dense_up, preferred_element_type=jnp.float32),
        ],
        axis=1,
    )
    dense_pre = lax.psum(dense_pre.astype(jnp.bfloat16), "tp").astype(jnp.float32)
    dense_pre_gate, dense_pre_up = jnp.split(dense_pre, 2, axis=1)
    dense_hidden = (jax.nn.silu(dense_pre_gate) * dense_pre_up).astype(jnp.bfloat16)
    dense_out = lax.psum_scatter(
        jnp.dot(dense_hidden, dense_down, preferred_element_type=jnp.float32).astype(jnp.bfloat16),
        "ep",
        scatter_dimension=0,
        tiled=True,
    ).astype(jnp.float32)
    route_width = routes.shape[1]
    expert_count = ep_count * expert_gate.shape[0]
    capacity = 2 * seq_local * route_width // ep_count
    flat_expert = routes.reshape(-1)
    picks = (flat_expert[:, None] == jnp.arange(expert_count, dtype=jnp.int32)[None, :]).astype(
        jnp.int32
    )
    ranks = jnp.sum(jnp.cumsum(picks, axis=0) * picks, axis=1) - 1
    slot_index = flat_expert * capacity + ranks
    placing = (
        jnp.arange(expert_count * capacity, dtype=jnp.int32)[:, None] == slot_index[None, :]
    ).astype(jnp.bfloat16)
    repeated = jnp.repeat(normed, route_width, axis=0)
    outgoing = (
        jnp.dot(placing, repeated, preferred_element_type=jnp.float32)
        .astype(jnp.bfloat16)
        .reshape(expert_count, capacity, part_width)
    )
    arrived = lax.all_to_all(outgoing, "ep", split_axis=0, concat_axis=0, tiled=True)
    full_rows = lax.all_gather(arrived, "tp", axis=2, tiled=True)
    flat_rows = full_rows.reshape(-1, width)
    gate_pre = jnp.dot(flat_rows, expert_gate[0], preferred_element_type=jnp.float32)
    up_pre = jnp.dot(flat_rows, expert_up[0], preferred_element_type=jnp.float32)
    hidden_units = (jax.nn.silu(gate_pre) * up_pre).astype(jnp.bfloat16)
    partial_out = settle(jnp.dot(hidden_units, expert_down[0], preferred_element_type=jnp.float32))
    summed_out = lax.psum_scatter(
        partial_out.astype(jnp.bfloat16), "tp", scatter_dimension=1, tiled=True
    )
    returned = lax.all_to_all(
        summed_out.reshape(arrived.shape), "ep", split_axis=0, concat_axis=0, tiled=True
    )
    picked = lax.dot_general(
        placing,
        returned.reshape(expert_count * capacity, part_width),
        (((0,), (0,)), ((), ())),
        preferred_element_type=jnp.float32,
    )
    share = route_scores / jnp.sum(route_scores, axis=-1, keepdims=True)
    moe_out = jnp.sum(
        picked.reshape(seq_local, route_width, part_width) * share[:, :, None], axis=1
    )
    ffn = moe_out + mix_gate[:, None] * dense_out
    ffn_sq = lax.psum(jnp.sum(ffn * ffn, axis=-1), "tp")
    new_hidden = (residual + gain_rows[3] * ffn * lax.rsqrt(ffn_sq / width + EPS)[:, None]).astype(
        jnp.bfloat16
    )
    return (new_hidden, new_matrix, new_norm, new_max)


def solution(mesh):
    placed = (
        P("ep", None),
        P(),
        P(None, "tp"),
        P(None, "tp"),
        P(None, "tp"),
        P(None, "tp"),
        P(),
        P(),
        P(),
        P("tp", None),
        P("ep", "tp", None, None),
        P("ep", "tp", None),
        P("ep", "tp"),
        P("ep", None),
        P("ep", None),
        P("ep", None, "tp"),
        P("ep", None, "tp"),
        P("ep", "tp", None),
        P("tp", "ep"),
        P("tp", "ep"),
        P("ep", "tp"),
        P(),
    )
    return jax.shard_map(
        local,
        mesh=mesh,
        in_specs=placed,
        out_specs=(P("ep", "tp"), P("ep", "tp", None, None), P("ep", "tp", None), P("ep", "tp")),
        check_vma=False,
    )
```

profile of v0, /device:TPU:0, one launch (start us, length us, event | category | flops | bytes accessed | tf_op | source)
XLA Modules:
  0.0 237.0 jit_solution(14512095781934341025)
XLA Ops:
  7.2 0.0 copy-start
  7.2 0.0 copy-start.2
  7.2 0.0 reduce-scatter.4.cloned.1.call-start
  7.3 0.9 slice.14
  8.2 1.0 multiply_reduce_fusion
  9.2 1.6 convolution_convert_fusion.7
  10.9 1.1 fusion.44
  12.0 0.7 dynamic_slice.21
  12.8 1.2 subtract_exponential_fusion
  13.9 0.0 copy-start.7
  14.0 0.1 copy.32
  14.0 0.1 copy.31
  14.1 1.6 convolution_convert_fusion.6
  15.8 1.6 convolution_convert_fusion.5
  17.5 0.8 fusion.38
  18.2 0.1 copy.42
  18.3 0.1 copy.34
  18.4 0.3 convolution_convert_fusion.8
  18.7 3.7 %multiply_add_fusion = f32[32,2,128,128]{3,2,1,0:T(8,128)S(1)} fusion(f32[32,2,128,128]{3,2,1,0:T(8,128)} %param.32, f32[32,2,128]{2,1,0:T(2,128)S(1)} %reshape.112, f32[32,2,128]{2,1,0:T(2,128)S(1)} %get-tuple-element.20, f32[32,2]{1,0:T(8,128)S(1)} %copy.31), kind=kLoop, calls=%fused_computation | loop fusion | flops 3145728 | bytes 8454400 | tf_op jit(solution)/shard_map/add | solution.py:72
  22.4 0.0 copy-start.1
  22.5 2.0 copy-done.1
  24.5 0.6 fusion.57
  25.1 0.1 broadcast_divide_fusion
  25.3 0.9 convolution_convert_fusion
  26.2 0.0 reduce-scatter.4.cloned.1.call-update
  26.2 0.1 copy.35
  26.3 0.1 reshape.104
  26.4 0.1 fusion.40
  26.5 0.1 reduce_window_sum.11
  26.6 0.2 select_reduce_fusion
  26.8 0.9 fusion.56
  27.7 0.8 dynamic-slice_multiply_fusion
  28.5 20.2 %reduce-scatter.4.cloned.1.call-done = bf16[32,512]{1,0:T(8,128)(2,1)} async-done(((bf16[32,2048]{1,0:T(8,128)(2,1)}), bf16[32,512]{1,0:T(8,128)(2,1)}) %reduce-scatter.4.cloned.1.call-update) | async-done | bytes 32784 | tf_op jit(solution)/shard_map/reduce_scatter | solution.py:83
  48.7 1.0 multiply_reduce_fusion.2
  49.7 5.8 %all-reduce = (f32[32]{0:T(128)S(1)}, f32[32]{0:T(128)S(1)}, f32[32]{0:T(128)S(1)}, f32[32]{0:T(128)S(1)}, f32[32]{0:T(128)S(1)}, /*index=5*/f32[32]{0:T(128)S(1)}) all-reduce(f32[32]{0:T(128)S(1)} %get-tuple-element.9, f32[32]{0:T(128)S(1)} %get-tuple-element.8, f32[32]{0:T(128)S(1)} %get-tuple-element.5, ...), channel_id=1, replica_groups=mesh['ep'=8,'tp'=4] {'tp'}, use_global_device_ids=true, to_apply=%region_3.4 | all-reduce | flops 192 | bytes 1536 | tf_op jit(solution)/shard_map/psum | solution.py:91
  55.5 0.9 multiply_convert_fusion.1
  56.3 31.2 %all_gather.7 = bf16[256,512]{1,0:T(8,128)(2,1)S(1)} all-gather(bf16[32,512]{1,0:T(8,128)(2,1)S(1)} %get-tuple-element.23), channel_id=1, replica_groups=mesh['ep'=8,'tp'=4] {'ep'}, dimensions={0}, use_global_device_ids=true | all-gather | bytes 294912 | tf_op jit(solution)/shard_map/all_gather | solution.py:110
  87.5 0.4 convolution_convert_fusion.1
  87.9 0.4 convolution_convert_fusion.2
  88.4 0.8 convolution_convert_fusion.4
  89.2 5.3 %all-to-all-start = ((bf16[8,16,512]{2,1,0:T(8,128)(2,1)}), bf16[8,16,512]{2,1,0:T(8,128)(2,1)S(1)}, u32[]{:S(2)}, u32[]{:S(2)}) async-start(bf16[8,16,512]{2,1,0:T(8,128)(2,1)} %bitcast.6), calls=%async_computation.1 | async-start | bytes 262144 | tf_op jit(solution)/shard_map/all_to_all | solution.py:145
  94.5 0.0 all-reduce.3.cloned.1.call-start
  94.5 0.9 pad_maximum_fusion
  95.4 0.0 all-reduce.3.cloned.1.call-update
  95.5 0.0 reduce-scatter.6.cloned.1.call-start
  95.5 6.3 %all-to-all-done = bf16[8,16,512]{2,1,0:T(8,128)(2,1)S(1)} async-done(((bf16[8,16,512]{2,1,0:T(8,128)(2,1)}), bf16[8,16,512]{2,1,0:T(8,128)(2,1)S(1)}, u32[]{:S(2)}, u32[]{:S(2)}) %all-to-all-start) | async-done | bytes 131104 | tf_op jit(solution)/shard_map/all_to_all | solution.py:145
  101.8 9.2 %all_gather.6 = bf16[8,16,2048]{2,1,0:T(8,128)(2,1)S(1)} all-gather(bf16[8,16,512]{2,1,0:T(8,128)(2,1)S(1)} %all-to-all-done), channel_id=1, replica_groups=mesh['ep'=8,'tp'=4] {'tp'}, dimensions={2}, use_global_device_ids=true | all-gather | bytes 655360 | tf_op jit(solution)/shard_map/all_gather | solution.py:146
  111.0 2.8 %fusion.4 = f32[128,896]{1,0:T(8,128)S(1)} fusion(bf16[128,2048]{1,0:T(8,128)(2,1)S(1)} %bitcast.51, bf16[1,2048,896]{2,1,0:T(8,128)(2,1)} %param.37), kind=kOutput, calls=%fused_computation.5 | convolution fusion | flops 469762048 | bytes 4653056 | tf_op jit(solution)/shard_map/dot_general | solution.py:148
  113.9 5.5 %fusion.6 = bf16[128,2048]{1,0:T(8,128)(2,1)} fusion(bf16[1,896,2048]{2,1,0:T(8,128)(2,1)} %param.39, bf16[128,2048]{1,0:T(8,128)(2,1)S(1)} %bitcast.52, bf16[1,2048,896]{2,1,0:T(8,128)(2,1)} %param.38, f32[128,896]{1,0:T(8,128)S(1)} %fusion.4), kind=kOutput, calls=%fused_computation.7 | convolution fusion | flops 940474368 | bytes 8847360 | tf_op jit(solution)/shard_map/dot_general | solution.py:151
  119.3 0.0 reduce-scatter.6.cloned.1.call-update
  119.3 0.0 reduce-scatter.8.cloned.1.call-start
  119.4 13.2 %all-reduce.3.cloned.1.call-done = bf16[256,1408]{0,1:T(8,128)(2,1)} async-done(((bf16[256,1408]{0,1:T(8,128)(2,1)}), bf16[256,1408]{0,1:T(8,128)(2,1)}) %all-reduce.3.cloned.1.call-update) | async-done | bytes 720912 | tf_op jit(solution)/shard_map/psum | solution.py:118
  132.6 1.2 convert_element_type.94
  133.8 1.1 convolution_convert_fusion.3
  134.9 0.0 reduce-scatter.8.cloned.1.call-update
  134.9 21.8 %reduce-scatter.6.cloned.1.call-done = bf16[128,512]{1,0:T(8,128)(2,1)} async-done(((bf16[128,2048]{1,0:T(8,128)(2,1)}), bf16[128,512]{1,0:T(8,128)(2,1)}) %reduce-scatter.6.cloned.1.call-update) | async-done | bytes 131088 | tf_op jit(solution)/shard_map/reduce_scatter | solution.py:152
  156.7 5.5 %all-to-all-start.1 = ((bf16[8,16,512]{2,1,0:T(8,128)(2,1)}), bf16[8,16,512]{2,1,0:T(8,128)(2,1)S(1)}, u32[]{:S(2)}, u32[]{:S(2)}) async-start(bf16[8,16,512]{2,1,0:T(8,128)(2,1)} %bitcast.62), calls=%async_computation.3 | async-start | bytes 262144 | tf_op jit(solution)/shard_map/all_to_all | solution.py:155
  162.3 0.1 iota_compare_fusion.3
  162.4 7.2 %all-to-all-done.1 = bf16[8,16,512]{2,1,0:T(8,128)(2,1)S(1)} async-done(((bf16[8,16,512]{2,1,0:T(8,128)(2,1)}), bf16[8,16,512]{2,1,0:T(8,128)(2,1)S(1)}, u32[]{:S(2)}, u32[]{:S(2)}) %all-to-all-start.1) | async-done | bytes 131104 | tf_op jit(solution)/shard_map/all_to_all | solution.py:155
  169.6 0.2 fusion.15
  169.8 52.6 %reduce-scatter.8.cloned.1.call-done = bf16[32,512]{1,0:T(8,128)(2,1)} async-done(((bf16[256,512]{1,0:T(8,128)(2,1)}), bf16[32,512]{1,0:T(8,128)(2,1)}) %reduce-scatter.8.cloned.1.call-update) | async-done | bytes 32784 | tf_op jit(solution)/shard_map/reduce_scatter | solution.py:121
  222.4 0.9 multiply_reduce_fusion.1
  223.3 5.7 %psum.63 = f32[32]{0:T(128)S(1)} all-reduce(f32[32]{0:T(128)S(1)} %multiply_reduce_fusion.1), channel_id=1, replica_groups=mesh['ep'=8,'tp'=4] {'tp'}, use_global_device_ids=true, to_apply=%region_22.23 | all-reduce | flops 32 | bytes 256 | tf_op jit(solution)/shard_map/psum | solution.py:169
  229.0 1.5 add_convert_fusion
  (33 shorter events, 0.3 us)
Async XLA Ops:
  7.2 18.1 %copy-start = (bf16[256,2048]{1,0:T(8,128)(2,1)S(1)}, bf16[256,2048]{1,0:T(8,128)(2,1)}, u32[]{:S(2)}) copy-start(bf16[256,2048]{1,0:T(8,128)(2,1)} %param.31) | copy-start | bytes 3145732
  7.2 11.2 %copy-start.2 = (bf16[32,2048]{1,0:T(8,128)(2,1)S(1)}, bf16[32,2048]{1,0:T(8,128)(2,1)}, u32[]{:S(2)}) copy-start(bf16[32,2048]{1,0:T(8,128)(2,1)} %param.22) | copy-start | bytes 393220
  7.2 10.3 %copy-start.6 = (f32[32,2,128]{2,1,0:T(2,128)S(1)}, f32[32,2,128]{2,1,0:T(2,128)}, u32[]{:S(2)}) copy-start(f32[32,2,128]{2,1,0:T(2,128)} %param.33) | copy-start | bytes 98308
  7.2 11.2 %copy-start.3 = (bf16[2048,256]{1,0:T(8,128)(2,1)S(1)}, bf16[2048,256]{1,0:T(8,128)(2,1)}, u32[]{:S(2)}) copy-start(bf16[2048,256]{1,0:T(8,128)(2,1)} %param.27) | copy-start | bytes 3145732
  7.2 41.5 %reduce-scatter.4.cloned.1.call-start = ((), (), s32[]{:S(2)}) async-start(), calls=%async_computation.5 | async-start | bytes 163840 | tf_op jit(solution)/shard_map/reduce_scatter | solution.py:83
  13.9 8.5 %copy-start.7 = (f32[32,2]{0,1:T(2,128)}, f32[32,2]{0,1:T(2,128)S(1)}, u32[]{:S(2)}) copy-start(f32[32,2]{0,1:T(2,128)S(1)} %get-tuple-element.22) | copy-start | bytes 772
  22.4 2.0 copy-start.1
  24.5 1.7 copy-start.9
  24.5 63.0 %copy-start.4 = (bf16[512,704]{0,1:T(8,128)(2,1)S(1)}, bf16[512,704]{0,1:T(8,128)(2,1)}, u32[]{:S(2)}) copy-start(bf16[512,704]{0,1:T(8,128)(2,1)} %param.41) | copy-start | bytes 2162692
  24.5 63.4 %copy-start.5 = (bf16[512,704]{0,1:T(8,128)(2,1)S(1)}, bf16[512,704]{0,1:T(8,128)(2,1)}, u32[]{:S(2)}) copy-start(bf16[512,704]{0,1:T(8,128)(2,1)} %param.40) | copy-start | bytes 2162692
  89.2 12.6 %all-to-all-start = ((bf16[8,16,512]{2,1,0:T(8,128)(2,1)}), bf16[8,16,512]{2,1,0:T(8,128)(2,1)S(1)}, u32[]{:S(2)}, u32[]{:S(2)}) async-start(bf16[8,16,512]{2,1,0:T(8,128)(2,1)} %bitcast.6), calls=%async_computation.1 | async-start | bytes 262144 | tf_op jit(solution)/shard_map/all_to_all | solution.py:145
  94.5 38.1 %all-reduce.3.cloned.1.call-start = ((), (), s32[]{:S(2)}) async-start(), calls=%async_computation.7 | async-start | bytes 1441792 | tf_op jit(solution)/shard_map/psum | solution.py:118
  95.5 61.3 %reduce-scatter.6.cloned.1.call-start = ((), (), s32[]{:S(2)}) async-start(), calls=%async_computation.6 | async-start | bytes 655360 | tf_op jit(solution)/shard_map/reduce_scatter | solution.py:152
  113.8 19.9 %copy-start.10 = (bf16[704,512]{1,0:T(8,128)(2,1)S(1)}, bf16[704,512]{1,0:T(8,128)(2,1)}, u32[]{:S(2)}) copy-start(bf16[704,512]{1,0:T(8,128)(2,1)} %param.42) | copy-start | bytes 2162692
  119.3 43.0 %copy-start.8 = (f32[32,2]{0,1:T(2,128)S(1)}, f32[32,2]{0,1:T(2,128)}, u32[]{:S(2)}) copy-start(f32[32,2]{0,1:T(2,128)} %param.36) | copy-start | bytes 772
  119.3 103.0 %reduce-scatter.8.cloned.1.call-start = ((), (), s32[]{:S(2)}) async-start(), calls=%async_computation.8 | async-start | bytes 294912 | tf_op jit(solution)/shard_map/reduce_scatter | solution.py:121
  156.7 12.9 %all-to-all-start.1 = ((bf16[8,16,512]{2,1,0:T(8,128)(2,1)}), bf16[8,16,512]{2,1,0:T(8,128)(2,1)S(1)}, u32[]{:S(2)}, u32[]{:S(2)}) async-start(bf16[8,16,512]{2,1,0:T(8,128)(2,1)} %bitcast.62), calls=%async_computation.3 | async-start | bytes 262144 | tf_op jit(solution)/shard_map/all_to_all | solution.py:155
Sparse Core Ops, SparseCore 0:
  26.3 22.3 reduce-scatter.3
  97.7 34.8 all-reduce.2
  135.0 21.6 reduce-scatter.5
  159.9 62.4 reduce-scatter.7
where the time goes:
time: 238 us; the launch traced here: 237 us
  waiting for transfers between devices  121 us (51%)
  blocking collectives  51.8 us (22%)
  matrix products  20.2 us (8%)
  between operations  14.1 us (6%)
  other arithmetic  13.3 us (6%)
  starting transfers between devices  11 us (5%)
  local copies, waits for them, and re-layouts  5.31 us (2%)
    reduce_scatter x1, waiting for transfers between devices, local(): lax.psum_scatter(jnp.dot(dense_hidden, dense_down, preferred_element_type...  52.6 us
    all_gather x1, blocking collectives, local(): rows_in = lax.all_gather(normed, 'ep', axis=0, tiled=True)  31.2 us
    reduce_scatter x1, waiting for transfers between devices, local(): lax.psum_scatter(partial_out.astype(jnp.bfloat16), 'tp', scatter_dimensio...  21.8 us
    reduce_scatter x1, waiting for transfers between devices, local(): lax.psum_scatter(branch_terms.astype(jnp.bfloat16), 'tp', scatter_dimensi...  20.2 us
    psum x1, waiting for transfers between devices, local(): lax.psum(dense_pre.astype(jnp.bfloat16), 'tp').astype(jnp.float32)  13.2 us
    all_gather x1, blocking collectives, local(): full_rows = lax.all_gather(arrived, 'tp', axis=2, tiled=True)  9.21 us
    all_to_all x1, waiting for transfers between devices, local(): lax.all_to_all(summed_out.reshape(arrived.shape), 'ep', split_axis=0, con...  7.21 us
    all_to_all x1, waiting for transfers between devices, local(): lax.all_to_all(outgoing, 'ep', split_axis=0, concat_axis=0, tiled=True)  6.31 us
  transfers between devices with their start and end apart: 6, of which 6 were waited for; matrix products, arithmetic and copies ran while one was open for 6% of the time, Pallas kernels for 0%

commit v1 on v0

--- a/solution.py
+++ b/solution.py
@@ -107,7 +107,9 @@
     mix_gate = jax.nn.sigmoid(scale_two * gate_dot)
     residual = settle(residual_f)
     normed = (residual_f * scale_two[:, None] * gain_rows[2]).astype(jnp.bfloat16)
-    rows_in = lax.all_gather(normed, "ep", axis=0, tiled=True)
+    rows_in = jnp.concatenate(
+        lax.all_to_all(jnp.stack([normed] * lax.axis_size("ep")), "ep", 0, 0), axis=0
+    )
     dense_pre = jnp.concatenate(
         [
             jnp.dot(rows_in, dense_gate, preferred_element_type=jnp.float32),

time: 238 us -> 226 us (0.950)
  blocking collectives: 51.8 us -> 30.7 us
  waiting for transfers between devices: 121 us -> 132 us
    all_gather x1 -> x0, blocking collectives: 31.2 us -> none  [local(): rows_in = lax.all_gather(normed, 'ep', axis=0, tiled=True)]
    psum x1, waiting for transfers between devices: 13.2 us -> 29.9 us  [local(): lax.psum(dense_pre.astype(jnp.bfloat16), 'tp').astype(jnp.float32)]
    all_to_all x0 -> x1, blocking collectives: none -> 12.8 us  [local(): lax.all_to_all(outgoing, 'ep', split_axis=0, concat_axis=0, tiled=True)]
    all_to_all x1, waiting for transfers between devices: 6.31 us -> 0.01 us  [local(): lax.all_to_all(jnp.stack([normed] * lax.axis_size('ep')), 'ep', 0, 0)]
    all_gather x1, blocking collectives: 9.21 us -> 6.5 us  [local(): full_rows = lax.all_gather(arrived, 'tp', axis=2, tiled=True)]
  transfers between devices with their start and end apart: 6 -> 6, of which waited for: 6 -> 5; matrix products, arithmetic and copies ran while one was open for 6% -> 6% of each run, Pallas kernels for 0% -> 0%
where the time goes in v1:
time: 226 us; the launch traced here: 225 us
  waiting for transfers between devices  132 us (58%)
  blocking collectives  30.7 us (14%)
  matrix products  20.3 us (9%)
  between operations  14.1 us (6%)
  other arithmetic  13.3 us (6%)
  starting transfers between devices  9.09 us (4%)
  local copies, waits for them, and re-layouts  6.02 us (3%)
    reduce_scatter x1, waiting for transfers between devices, local(): lax.psum_scatter(jnp.dot(dense_hidden, dense_down, preferred_element_type...  52.6 us
    psum x1, waiting for transfers between devices, local(): lax.psum(dense_pre.astype(jnp.bfloat16), 'tp').astype(jnp.float32)  29.9 us
    reduce_scatter x1, waiting for transfers between devices, local(): lax.psum_scatter(partial_out.astype(jnp.bfloat16), 'tp', scatter_dimensio...  21.8 us
    reduce_scatter x1, waiting for transfers between devices, local(): lax.psum_scatter(branch_terms.astype(jnp.bfloat16), 'tp', scatter_dimensi...  20.2 us
    all_to_all x1, blocking collectives, local(): lax.all_to_all(outgoing, 'ep', split_axis=0, concat_axis=0, tiled=True)  12.8 us
    all_to_all x1, waiting for transfers between devices, local(): lax.all_to_all(summed_out.reshape(arrived.shape), 'ep', split_axis=0, con...  7.21 us
    all_gather x1, blocking collectives, local(): full_rows = lax.all_gather(arrived, 'tp', axis=2, tiled=True)  6.5 us
    psum x1, blocking collectives, local(): lax.psum((jnp.sum(branch * branch, axis=-1), jnp.sum(start_part * start_p...  5.77 us
  transfers between devices with their start and end apart: 6, of which 5 were waited for; matrix products, arithmetic and copies ran while one was open for 6% of the time, Pallas kernels for 0%

profile of v1, /device:TPU:0, one launch (start us, length us, event | category | flops | bytes accessed | tf_op | source)
XLA Modules:
  0.0 225.4 jit_solution(14164647654718429475)
XLA Ops:
  7.2 0.0 copy-start
  7.2 0.0 copy-start.2
  7.2 0.0 reduce-scatter.4.cloned.1.call-start
  7.3 0.9 slice.14
  8.2 1.0 multiply_reduce_fusion
  9.2 1.6 convolution_convert_fusion.7
  10.9 1.1 fusion.44
  12.0 0.7 dynamic_slice.21
  12.8 1.2 subtract_exponential_fusion
  13.9 0.0 copy-start.7
  14.0 0.1 copy.32
  14.0 0.1 copy.31
  14.1 1.6 convolution_convert_fusion.6
  15.8 1.6 convolution_convert_fusion.5
  17.5 0.8 fusion.38
  18.2 0.1 copy.42
  18.3 0.1 copy.34
  18.4 0.3 convolution_convert_fusion.8
  18.7 3.7 %multiply_add_fusion = f32[32,2,128,128]{3,2,1,0:T(8,128)S(1)} fusion(f32[32,2,128,128]{3,2,1,0:T(8,128)} %param.32, f32[32,2,128]{2,1,0:T(2,128)S(1)} %reshape.118, f32[32,2,128]{2,1,0:T(2,128)S(1)} %get-tuple-element.20, f32[32,2]{1,0:T(8,128)S(1)} %copy.31), kind=kLoop, calls=%fused_computation | loop fusion | flops 3145728 | bytes 8454400 | tf_op jit(solution)/shard_map/add | solution.py:72
  22.5 0.0 copy-start.1
  22.5 2.0 copy-done.1
  24.5 0.6 fusion.57
  25.1 0.1 broadcast_divide_fusion
  25.2 0.9 convolution_convert_fusion
  26.2 0.0 reduce-scatter.4.cloned.1.call-update
  26.2 0.1 copy.35
  26.3 0.1 reshape.109
  26.4 0.1 fusion.40
  26.5 0.1 reduce_window_sum.11
  26.6 0.2 select_reduce_fusion
  26.8 0.9 fusion.56
  27.7 0.8 dynamic-slice_multiply_fusion
  28.5 20.2 %reduce-scatter.4.cloned.1.call-done = bf16[32,512]{1,0:T(8,128)(2,1)} async-done(((bf16[32,2048]{1,0:T(8,128)(2,1)}), bf16[32,512]{1,0:T(8,128)(2,1)}) %reduce-scatter.4.cloned.1.call-update) | async-done | bytes 32784 | tf_op jit(solution)/shard_map/reduce_scatter | solution.py:83
  48.7 1.0 multiply_reduce_fusion.2
  49.7 5.8 %all-reduce = (f32[32]{0:T(128)S(1)}, f32[32]{0:T(128)S(1)}, f32[32]{0:T(128)S(1)}, f32[32]{0:T(128)S(1)}, f32[32]{0:T(128)S(1)}, /*index=5*/f32[32]{0:T(128)S(1)}) all-reduce(f32[32]{0:T(128)S(1)} %get-tuple-element.9, f32[32]{0:T(128)S(1)} %get-tuple-element.8, f32[32]{0:T(128)S(1)} %get-tuple-element.5, ...), channel_id=1, replica_groups=mesh['ep'=8,'tp'=4] {'tp'}, use_global_device_ids=true, to_apply=%region_3.4 | all-reduce | flops 192 | bytes 1536 | tf_op jit(solution)/shard_map/psum | solution.py:91
  55.5 0.9 multiply_convert_fusion.1
  56.4 0.2 convolution_convert_fusion.4
  56.6 12.8 %all_to_all.15 = bf16[8,16,512]{2,1,0:T(8,128)(2,1)S(1)} all-to-all(bf16[8,16,512]{2,1,0:T(8,128)(2,1)S(1)} %bitcast.57), channel_id=1, replica_groups=mesh['ep'=8,'tp'=4] {'ep'}, dimensions={0} | all-to-all | bytes 262144 | tf_op jit(solution)/shard_map/all_to_all | solution.py:147
  69.4 0.7 stack.2
  70.1 3.4 %all-to-all-start.2 = ((bf16[8,32,512]{2,1,0:T(8,128)(2,1)}), bf16[8,32,512]{2,1,0:T(8,128)(2,1)S(1)}, u32[]{:S(2)}, u32[]{:S(2)}) async-start(bf16[8,32,512]{2,1,0:T(8,128)(2,1)} %stack.2), calls=%async_computation.4 | async-start | bytes 524288 | tf_op jit(solution)/shard_map/all_to_all | solution.py:111
  73.5 0.0 all-reduce.3.cloned.1.call-start
  73.6 6.5 %all_gather.3 = bf16[8,16,2048]{2,1,0:T(8,128)(2,1)S(1)} all-gather(bf16[8,16,512]{2,1,0:T(8,128)(2,1)S(1)} %all_to_all.15), channel_id=1, replica_groups=mesh['ep'=8,'tp'=4] {'tp'}, dimensions={2}, use_global_device_ids=true | all-gather | bytes 655360 | tf_op jit(solution)/shard_map/all_gather | solution.py:148
  80.1 3.6 %fusion.4 = f32[128,896]{1,0:T(8,128)} fusion(bf16[128,2048]{1,0:T(8,128)(2,1)S(1)} %bitcast.54, bf16[1,2048,896]{2,1,0:T(8,128)(2,1)} %param.37), kind=kOutput, calls=%fused_computation.5 | convolution fusion | flops 469762048 | bytes 4653056 | tf_op jit(solution)/shard_map/dot_general | solution.py:150
  83.6 0.4 convolution_convert_fusion.1
  84.0 0.4 convolution_convert_fusion.2
  84.4 0.9 pad_maximum_fusion
  85.3 0.0 all-reduce.3.cloned.1.call-update
  85.4 0.0 reduce-scatter.6.cloned.1.call-start
  85.4 5.5 %fusion.6 = bf16[128,2048]{1,0:T(8,128)(2,1)} fusion(bf16[1,896,2048]{2,1,0:T(8,128)(2,1)} %param.39, bf16[128,2048]{1,0:T(8,128)(2,1)S(1)} %bitcast.55, bf16[1,2048,896]{2,1,0:T(8,128)(2,1)} %param.38, f32[128,896]{1,0:T(8,128)} %fusion.4), kind=kOutput, calls=%fused_computation.7 | convolution fusion | flops 940474368 | bytes 8847360 | tf_op jit(solution)/shard_map/dot_general | solution.py:153
  90.9 0.0 reduce-scatter.6.cloned.1.call-update
  90.9 0.0 reduce-scatter.8.cloned.1.call-start
  91.0 29.9 %all-reduce.3.cloned.1.call-done = bf16[256,1408]{0,1:T(8,128)(2,1)} async-done(((bf16[256,1408]{0,1:T(8,128)(2,1)}), bf16[256,1408]{0,1:T(8,128)(2,1)}) %all-reduce.3.cloned.1.call-update) | async-done | bytes 720912 | tf_op jit(solution)/shard_map/psum | solution.py:120
  120.9 1.2 convert_element_type.94
  122.2 1.1 convolution_convert_fusion.3
  123.3 0.0 reduce-scatter.8.cloned.1.call-update
  123.3 21.8 %reduce-scatter.6.cloned.1.call-done = bf16[128,512]{1,0:T(8,128)(2,1)} async-done(((bf16[128,2048]{1,0:T(8,128)(2,1)}), bf16[128,512]{1,0:T(8,128)(2,1)}) %reduce-scatter.6.cloned.1.call-update) | async-done | bytes 131088 | tf_op jit(solution)/shard_map/reduce_scatter | solution.py:154
  145.1 5.5 %all-to-all-start.1 = ((bf16[8,16,512]{2,1,0:T(8,128)(2,1)}), bf16[8,16,512]{2,1,0:T(8,128)(2,1)S(1)}, u32[]{:S(2)}, u32[]{:S(2)}) async-start(bf16[8,16,512]{2,1,0:T(8,128)(2,1)} %bitcast.66), calls=%async_computation.3 | async-start | bytes 262144 | tf_op jit(solution)/shard_map/all_to_all | solution.py:157
  150.6 0.1 iota_compare_fusion.3
  150.8 7.2 %all-to-all-done.1 = bf16[8,16,512]{2,1,0:T(8,128)(2,1)S(1)} async-done(((bf16[8,16,512]{2,1,0:T(8,128)(2,1)}), bf16[8,16,512]{2,1,0:T(8,128)(2,1)S(1)}, u32[]{:S(2)}, u32[]{:S(2)}) %all-to-all-start.1) | async-done | bytes 131104 | tf_op jit(solution)/shard_map/all_to_all | solution.py:157
  158.0 0.2 fusion.15
  158.1 52.6 %reduce-scatter.8.cloned.1.call-done = bf16[32,512]{1,0:T(8,128)(2,1)} async-done(((bf16[256,512]{1,0:T(8,128)(2,1)}), bf16[32,512]{1,0:T(8,128)(2,1)}) %reduce-scatter.8.cloned.1.call-update) | async-done | bytes 32784 | tf_op jit(solution)/shard_map/reduce_scatter | solution.py:123
  210.8 0.9 multiply_reduce_fusion.1
  211.7 5.7 %psum.63 = f32[32]{0:T(128)S(1)} all-reduce(f32[32]{0:T(128)S(1)} %multiply_reduce_fusion.1), channel_id=1, replica_groups=mesh['ep'=8,'tp'=4] {'tp'}, use_global_device_ids=true, to_apply=%region_22.23 | all-reduce | flops 32 | bytes 256 | tf_op jit(solution)/shard_map/psum | solution.py:171
  217.4 1.5 add_convert_fusion
  (34 shorter events, 0.3 us)
Async XLA Ops:
  7.2 18.1 %copy-start = (bf16[256,2048]{1,0:T(8,128)(2,1)S(1)}, bf16[256,2048]{1,0:T(8,128)(2,1)}, u32[]{:S(2)}) copy-start(bf16[256,2048]{1,0:T(8,128)(2,1)} %param.31) | copy-start | bytes 3145732
  7.2 11.2 %copy-start.2 = (bf16[32,2048]{1,0:T(8,128)(2,1)S(1)}, bf16[32,2048]{1,0:T(8,128)(2,1)}, u32[]{:S(2)}) copy-start(bf16[32,2048]{1,0:T(8,128)(2,1)} %param.22) | copy-start | bytes 393220
  7.2 10.3 %copy-start.6 = (f32[32,2,128]{2,1,0:T(2,128)S(1)}, f32[32,2,128]{2,1,0:T(2,128)}, u32[]{:S(2)}) copy-start(f32[32,2,128]{2,1,0:T(2,128)} %param.33) | copy-start | bytes 98308
  7.2 11.2 %copy-start.3 = (bf16[2048,256]{1,0:T(8,128)(2,1)S(1)}, bf16[2048,256]{1,0:T(8,128)(2,1)}, u32[]{:S(2)}) copy-start(bf16[2048,256]{1,0:T(8,128)(2,1)} %param.27) | copy-start | bytes 3145732
  7.2 41.5 %reduce-scatter.4.cloned.1.call-start = ((), (), s32[]{:S(2)}) async-start(), calls=%async_computation.6 | async-start | bytes 163840 | tf_op jit(solution)/shard_map/reduce_scatter | solution.py:83
  13.9 8.5 %copy-start.7 = (f32[32,2]{0,1:T(2,128)}, f32[32,2]{0,1:T(2,128)S(1)}, u32[]{:S(2)}) copy-start(f32[32,2]{0,1:T(2,128)S(1)} %get-tuple-element.22) | copy-start | bytes 772
  22.5 2.0 copy-start.1
  24.5 1.7 copy-start.9
  27.7 56.0 %copy-start.4 = (bf16[512,704]{0,1:T(8,128)(2,1)S(1)}, bf16[512,704]{0,1:T(8,128)(2,1)}, u32[]{:S(2)}) copy-start(bf16[512,704]{0,1:T(8,128)(2,1)} %param.41) | copy-start | bytes 2162692
  69.4 14.6 %copy-start.5 = (bf16[512,704]{0,1:T(8,128)(2,1)S(1)}, bf16[512,704]{0,1:T(8,128)(2,1)}, u32[]{:S(2)}) copy-start(bf16[512,704]{0,1:T(8,128)(2,1)} %param.40) | copy-start | bytes 2162692
  70.1 13.5 %all-to-all-start.2 = ((bf16[8,32,512]{2,1,0:T(8,128)(2,1)}), bf16[8,32,512]{2,1,0:T(8,128)(2,1)S(1)}, u32[]{:S(2)}, u32[]{:S(2)}) async-start(bf16[8,32,512]{2,1,0:T(8,128)(2,1)} %stack.2), calls=%async_computation.4 | async-start | bytes 524288 | tf_op jit(solution)/shard_map/all_to_all | solution.py:111
  73.5 47.4 %all-reduce.3.cloned.1.call-start = ((), (), s32[]{:S(2)}) async-start(), calls=%async_computation.8 | async-start | bytes 1441792 | tf_op jit(solution)/shard_map/psum | solution.py:120
  85.4 36.8 %copy-start.10 = (bf16[704,512]{1,0:T(8,128)(2,1)S(1)}, bf16[704,512]{1,0:T(8,128)(2,1)}, u32[]{:S(2)}) copy-start(bf16[704,512]{1,0:T(8,128)(2,1)} %param.42) | copy-start | bytes 2162692
  85.4 59.7 %reduce-scatter.6.cloned.1.call-start = ((), (), s32[]{:S(2)}) async-start(), calls=%async_computation.7 | async-start | bytes 655360 | tf_op jit(solution)/shard_map/reduce_scatter | solution.py:154
  90.9 59.8 %copy-start.8 = (f32[32,2]{0,1:T(2,128)S(1)}, f32[32,2]{0,1:T(2,128)}, u32[]{:S(2)}) copy-start(f32[32,2]{0,1:T(2,128)} %param.36) | copy-start | bytes 772
  90.9 119.8 %reduce-scatter.8.cloned.1.call-start = ((), (), s32[]{:S(2)}) async-start(), calls=%async_computation.9 | async-start | bytes 294912 | tf_op jit(solution)/shard_map/reduce_scatter | solution.py:123
  145.1 12.9 %all-to-all-start.1 = ((bf16[8,16,512]{2,1,0:T(8,128)(2,1)}), bf16[8,16,512]{2,1,0:T(8,128)(2,1)S(1)}, u32[]{:S(2)}, u32[]{:S(2)}) async-start(bf16[8,16,512]{2,1,0:T(8,128)(2,1)} %bitcast.66), calls=%async_computation.3 | async-start | bytes 262144 | tf_op jit(solution)/shard_map/all_to_all | solution.py:157
Sparse Core Ops, SparseCore 0:
  26.3 22.3 reduce-scatter.3
  85.5 35.3 all-reduce.2
  123.4 21.6 reduce-scatter.5
  148.3 62.4 reduce-scatter.7
